TPU v7x, 32 devices: a whole 2x2x4 slice. The times are simulated.
32 devices in a mesh: sp: 8 (over z, core), tp: 4 (over y, x).
Axes of the slice: x: 2, y: 2, z: 4, core: 2. Of those that a mesh axis runs over, the one named last changes fastest.
Arguments:
- queries: bfloat16 [2048, 1024], P('sp', 'tp'), may hold values from -250 to 250
- keys_values: bfloat16 [2, 2048, 256], P(None, 'sp'), may hold values from -8 to 8
- sink_logits: float32 [16], P('tp'), may hold values from 1 to 5
- proj_weight: bfloat16 [1024, 2048], P('tp'), may hold values from -0.75 to 0.75
- residual: bfloat16 [2048, 2048], P('sp', 'tp'), may hold values from -6 to 6
- norm_gain: float32 [2048], replicated, may hold values from 0.1 to 1.9
- routes: int32 [2048, 2], P('sp'), may hold values from 0 to 7, all different within a row; in each aligned block of 256 rows (0 to 255, 256 to 511, ...) at most 128 rows name the same one
- route_weights: float32 [2048, 2], P('sp'), may hold values from 0.2 to 1
- gate_weight: bfloat16 [8, 2048, 2048], P('sp', None, 'tp'), may hold values from -0.125 to 0.125
- up_weight: bfloat16 [8, 2048, 2048], P('sp', None, 'tp'), may hold values from -0.125 to 0.125
- down_weight: bfloat16 [8, 2048, 2048], P('sp', None, 'tp'), may hold values from -0.125 to 0.125
- shared_gate: bfloat16 [2048, 2048], P(None, 'tp'), may hold values from -0.125 to 0.125
- shared_up: bfloat16 [2048, 2048], P(None, 'tp'), may hold values from -0.125 to 0.125
- shared_down: bfloat16 [2048, 2048], P(None, 'tp'), may hold values from -0.125 to 0.125
Outputs:
- output: bfloat16 [2048, 2048], P('sp', 'tp')
Inputs may be any that keep to these rules, and one draw needn't show every extreme that they name: `routes`: the 2 experts of a position differ. In each aligned block of 256 positions no expert is named by more than 128 positions, and in some block one expert is named by exactly 128.
All inputs are finite; a program needn't handle non-finite values.
Results may differ from a plain program's by a relative error of at most 0.0067.
Values may be sent and summed in bfloat16 or wider, within the bound.
A program may use at most 64 MiB of HBM per device.

v0:
```python
import jax
import jax.numpy as jnp
from jax import lax
from jax.sharding import PartitionSpec as P

D = 2048
HEADS = 16
KV_HEADS = 4
HEAD_WIDTH = 64
WINDOW = 128
TOP_K = 2
EXP_DEV = 1
TOK_DEV = 256
norm_eps = 1e-06


def passed_along(value, axis, steps):
    count = lax.axis_size(axis)
    initial, last = (max(0, -steps), min(count, count - steps))
    return lax.ppermute(value, axis, [(source, source + steps) for source in range(initial, last)])


def per_device(
    queries,
    keys_values,
    sink_logits,
    proj_weight,
    residual,
    norm_gain,
    routes,
    route_weights,
    gate_weight,
    up_weight,
    down_weight,
    shared_gate,
    shared_up,
    shared_down,
):
    tp_index = lax.axis_index("tp")
    sp_index = lax.axis_index("sp")
    sp_count = lax.axis_size("sp")
    tp_count = lax.axis_size("tp")
    heads_here = sink_logits.shape[0]
    col_width = residual.shape[1]
    blocks = TOK_DEV // WINDOW
    kv_group = HEADS // KV_HEADS
    earlier_keys = passed_along(keys_values[:, TOK_DEV - WINDOW :, :], "sp", 1)
    extended = jnp.concatenate([earlier_keys, keys_values], axis=1)
    extended = extended.reshape(2, TOK_DEV + WINDOW, KV_HEADS, HEAD_WIDTH)
    head_ids = tp_index * heads_here + jnp.arange(heads_here, dtype=jnp.int32)
    chosen = jnp.take(extended, head_ids // kv_group, axis=2)
    earlier = chosen[:, :TOK_DEV].reshape(2, blocks, WINDOW, heads_here, HEAD_WIDTH)
    later = chosen[:, WINDOW:].reshape(2, blocks, WINDOW, heads_here, HEAD_WIDTH)
    banded = jnp.concatenate([earlier, later], axis=2)
    query_blocks = queries.reshape(blocks, WINDOW, heads_here, HEAD_WIDTH)
    score_matrix = jnp.einsum(
        "bqhd,bkhd->bhqk", query_blocks, banded[0], preferred_element_type=jnp.float32
    ) * HEAD_WIDTH ** (-0.5)
    query_pos = jnp.arange(WINDOW, dtype=jnp.int32)[:, None]
    key_pos = jnp.arange(2 * WINDOW, dtype=jnp.int32)[None, :]
    distance = WINDOW + query_pos - key_pos
    absolute = (
        sp_index * TOK_DEV
        + jnp.arange(blocks, dtype=jnp.int32)[:, None, None] * WINDOW
        - WINDOW
        + key_pos[None]
    )
    allowed = (distance >= 0)[None] & (distance < WINDOW)[None] & (absolute >= 0)
    masked = jnp.where(allowed[:, None], score_matrix, -jnp.inf)
    sink_value = sink_logits[None, :, None, None]
    highest = jnp.maximum(jnp.max(masked, axis=-1, keepdims=True), sink_value)
    weights_exp = jnp.exp(masked - highest)
    denominator = jnp.sum(weights_exp, axis=-1, keepdims=True) + jnp.exp(sink_value - highest)
    softmax_weights = (weights_exp / denominator).astype(jnp.bfloat16)
    attended_values = jnp.einsum(
        "bhqk,bkhd->bqhd", softmax_weights, banded[1], preferred_element_type=jnp.float32
    )
    attended_values = attended_values.astype(jnp.bfloat16).reshape(TOK_DEV, heads_here * HEAD_WIDTH)
    attended_all = lax.all_gather(attended_values, "tp", axis=1, tiled=True)
    weight_rows = proj_weight.shape[0]
    column_share = lax.all_to_all(
        proj_weight.reshape(weight_rows, tp_count, col_width),
        "tp",
        split_axis=1,
        concat_axis=0,
        tiled=True,
    )
    column_share = column_share.reshape(HEADS * HEAD_WIDTH, col_width)
    feature_sum = jnp.dot(attended_all, column_share, preferred_element_type=jnp.float32)
    stream_cols = (feature_sum + residual.astype(jnp.float32)).astype(jnp.bfloat16)
    stream_rows = lax.all_gather(stream_cols, "tp", axis=1, tiled=True)
    gate_eff = (norm_gain[None, :, None] * gate_weight.astype(jnp.float32)).astype(jnp.bfloat16)
    up_eff = (norm_gain[None, :, None] * up_weight.astype(jnp.float32)).astype(jnp.bfloat16)
    shared_gate_eff = (norm_gain[:, None] * shared_gate.astype(jnp.float32)).astype(jnp.bfloat16)
    shared_up_eff = (norm_gain[:, None] * shared_up.astype(jnp.float32)).astype(jnp.bfloat16)
    experts_total = EXP_DEV * sp_count
    capacity = 2 * TOK_DEV * TOP_K // experts_total
    rows_per_expert = sp_count * capacity
    flat_routes = routes.reshape(-1)
    onehot = (flat_routes[:, None] == jnp.arange(experts_total, dtype=jnp.int32)[None, :]).astype(
        jnp.int32
    )
    before = jnp.cumsum(onehot, axis=0) - onehot
    slot_rank = jnp.sum(before * onehot, axis=1)
    slot_index = (
        flat_routes % EXP_DEV * rows_per_expert + flat_routes // EXP_DEV * capacity + slot_rank
    )
    token_of = jnp.arange(TOK_DEV * TOP_K, dtype=jnp.int32) // TOP_K
    slot_owner = (
        jnp.full((EXP_DEV * rows_per_expert,), TOK_DEV, jnp.int32).at[slot_index].set(token_of)
    )
    picked_rows = jnp.take(stream_rows, slot_owner, axis=0, mode="fill", fill_value=0)
    arrived = lax.all_to_all(
        picked_rows.reshape(EXP_DEV, sp_count, capacity, stream_rows.shape[1]),
        "sp",
        split_axis=1,
        concat_axis=1,
        tiled=True,
    )
    arrived = arrived.reshape(EXP_DEV, rows_per_expert, D)
    routed_squares = jnp.sum(jnp.square(arrived.astype(jnp.float32)), axis=-1)
    gate_sum = jnp.einsum("erd,edf->erf", arrived, gate_eff, preferred_element_type=jnp.float32)
    up_sum = jnp.einsum("erd,edf->erf", arrived, up_eff, preferred_element_type=jnp.float32)
    own_squares = jnp.sum(jnp.square(stream_rows.astype(jnp.float32)), axis=-1)
    shared_gate_sum = jnp.dot(stream_rows, shared_gate_eff, preferred_element_type=jnp.float32)
    shared_up_sum = jnp.dot(stream_rows, shared_up_eff, preferred_element_type=jnp.float32)
    routed_scale = lax.rsqrt(routed_squares / D + norm_eps)[..., None]
    own_scale = lax.rsqrt(own_squares / D + norm_eps)[:, None]
    hidden = (jax.nn.silu(routed_scale * gate_sum) * (routed_scale * up_sum)).astype(jnp.bfloat16)
    shared_hidden = (jax.nn.silu(own_scale * shared_gate_sum) * (own_scale * shared_up_sum)).astype(
        jnp.bfloat16
    )
    routed_piece = lax.all_gather(hidden, "tp", axis=2, tiled=True)
    own_piece = lax.all_gather(shared_hidden[None], "tp", axis=2, tiled=True)
    expert_out = jnp.einsum(
        "erf,efd->erd", routed_piece, down_weight, preferred_element_type=jnp.float32
    )
    shared_out = jnp.dot(own_piece[0], shared_down, preferred_element_type=jnp.float32)
    outgoing = expert_out.astype(jnp.bfloat16).reshape(EXP_DEV, sp_count, capacity, col_width)
    returned = lax.all_to_all(outgoing, "sp", split_axis=1, concat_axis=1, tiled=True).reshape(
        EXP_DEV * rows_per_expert, col_width
    )
    picked = jnp.take(returned, slot_index, axis=0).reshape(TOK_DEV, TOP_K, col_width)
    routed_sum = jnp.einsum("nk,nkd->nd", route_weights, picked.astype(jnp.float32))
    return (stream_cols.astype(jnp.float32) + shared_out + routed_sum).astype(jnp.bfloat16)


def solution(mesh):
    placed = (
        P("sp", "tp"),
        P(None, "sp", None),
        P("tp"),
        P("tp", None),
        P("sp", "tp"),
        P(),
        P("sp", None),
        P("sp", None),
        P("sp", None, "tp"),
        P("sp", None, "tp"),
        P("sp", None, "tp"),
        P(None, "tp"),
        P(None, "tp"),
        P(None, "tp"),
    )
    return jax.shard_map(
        per_device, mesh=mesh, in_specs=placed, out_specs=P("sp", "tp"), check_vma=False
    )
```

profile of v0, /device:TPU:0, one launch (start us, length us, event | category | flops | bytes accessed | tf_op | source)
XLA Modules:
  0.0 293.3 jit_solution(9455327325811044780)
XLA Ops:
  6.5 1.2 copy.63
  7.8 3.2 %collective-permute-start = (bf16[2,128,256]{1,2,0:T(8,128)(2,1)S(1)}, bf16[2,128,256]{1,2,0:T(8,128)(2,1)}, u32[]{:S(2)}, u32[]{:S(2)}) collective-permute-start(bf16[2,128,256]{1,2,0:T(8,128)(2,1)S(1)} %slice.34), channel_id=1, source_target_pairs={{0,4},{4,8},{8,12},{12,16},{16,20},{20,24},{24,28},{1,5},{5,9},{9,... | collective-permute-start | bytes 393224 | tf_op jit(solution)/shard_map/ppermute | solution.py:20
  11.0 2.3 copy.73
  13.3 4.5 %all-to-all-start = ((bf16[256,4,512]{0,2,1:T(8,128)(2,1)}), bf16[256,4,512]{0,2,1:T(8,128)(2,1)S(1)}, u32[]{:S(2)}, u32[]{:S(2)}) async-start(bf16[256,4,512]{0,2,1:T(8,128)(2,1)} %bitcast.91), calls=%async_computation | async-start | bytes 2097152 | tf_op jit(solution)/shard_map/all_to_all | solution.py:81
  18.7 0.9 reshape.384
  19.6 1.0 pad_maximum_fusion
  20.7 1.4 gather_fusion
  22.0 1.1 select_bitcast_fusion
  24.0 1.0 reshape.382
  25.8 1.0 reshape.383
  27.6 1.5 fusion.48
  30.0 12.7 %all_gather.12 = bf16[256,1024]{0,1:T(8,128)(2,1)} all-gather(bf16[256,256]{0,1:T(8,128)(2,1)S(1)} %bitcast.95), channel_id=1, replica_groups=mesh['sp'=8,'tp'=4] {'tp'}, dimensions={1}, use_global_device_ids=true | all-gather | bytes 655360 | tf_op jit(solution)/shard_map/all_gather | solution.py:79
  42.7 1.3 copy.74
  44.0 2.6 fusion.25
  47.1 1.1 reduce-window.6
  48.9 2.4 scatter_custom_fusion
  51.4 20.4 %all-gather.6.cloned.1.call-done = bf16[256,2048]{1,0:T(8,128)(2,1)} async-done(((bf16[256,512]{1,0:T(8,128)(2,1)}), bf16[256,2048]{1,0:T(8,128)(2,1)}) %all-gather.6.cloned.1.call-update) | async-done | bytes 1048592 | tf_op jit(solution)/shard_map/all_gather | solution.py:91
  71.8 10.2 %gather_fusion.1 = bf16[1024,2048]{1,0:T(8,128)(2,1)} fusion(bf16[256,2048]{1,0:T(8,128)(2,1)} %all-gather.6.cloned.1.call-done, s32[1024]{0:T(1024)S(1)} %fusion.39), kind=kCustom, calls=%fused_computation.1 | custom fusion | bytes 8392704 | tf_op jit(solution)/shard_map/jit(_take)/gather | solution.py:112
  82.0 2.5 broadcast_select_fusion
  84.5 98.4 %all_to_all.25 = bf16[1,8,128,2048]{3,2,0,1:T(8,128)(2,1)S(1)} all-to-all(bf16[1,8,128,2048]{3,2,0,1:T(8,128)(2,1)S(1)} %broadcast_select_fusion), channel_id=1, replica_groups=mesh['sp'=8,'tp'=4] {'sp'}, dimensions={1} | all-to-all | bytes 8388608 | tf_op jit(solution)/shard_map/all_to_all | solution.py:113
  182.9 0.9 multiply_reduce_fusion
  184.5 2.4 fusion.3
  186.9 3.7 %multiply_convert_fusion.6 = bf16[1024,512]{1,0:T(8,128)(2,1)} fusion(f32[1024,512]{1,0:T(8,128)S(1)} %fusion.3, bf16[1024,2048]{1,0:T(8,128)(2,1)S(1)} %bitcast.89, bf16[1,2048,512]{2,1,0:T(8,128)(2,1)S(1)} %copy-done.11, f32[2048]{0:T(1024)S(1)} %copy-done.14, f32[1024]{0:T(1024)S(1)} %rsqrt_bitcast_fusion), kind=kOutput, calls=%fused_computation.18 | convolution fusion | flops 2154823680 | bytes 9449472 | tf_op jit(solution)/shard_map/erd,edf->erf/dot_general | solution.py:123
  191.0 50.3 %all-gather.10.cloned.1.call-done = bf16[1024,2048]{1,0:T(8,128)(2,1)} async-done(((bf16[1024,512]{1,0:T(8,128)(2,1)}), bf16[1024,2048]{1,0:T(8,128)(2,1)}) %all-gather.10.cloned.1.call-update) | async-done | bytes 4194320 | tf_op jit(solution)/shard_map/all_gather | solution.py:133
  241.3 5.5 %fusion.16 = bf16[1024,512]{1,0:T(8,128)(2,1)} fusion(bf16[1024,2048]{1,0:T(8,128)(2,1)} %all-gather.10.cloned.1.call-done, bf16[1,2048,512]{2,1,0:T(8,128)(2,1)S(1)} %copy-done), kind=kOutput, calls=%fused_computation.24 | convolution fusion | flops 2148007936 | bytes 7340032 | tf_op jit(solution)/shard_map/erf,efd->erd/dot_general | solution.py:135
  246.8 4.6 %all-to-all-start.2 = ((bf16[1,8,128,512]{3,2,0,1:T(8,128)(2,1)}), bf16[1,8,128,512]{3,2,0,1:T(8,128)(2,1)}, u32[]{:S(2)}, u32[]{:S(2)}) async-start(bf16[1,8,128,512]{3,2,0,1:T(8,128)(2,1)} %bitcast.93), calls=%async_computation.2 | async-start | bytes 2097152 | tf_op jit(solution)/shard_map/all_to_all | solution.py:140
  251.4 2.6 fusion.23
  254.0 1.6 fusion.27
  256.3 21.8 %all-to-all-done.2 = bf16[1,8,128,512]{3,2,0,1:T(8,128)(2,1)} async-done(((bf16[1,8,128,512]{3,2,0,1:T(8,128)(2,1)}), bf16[1,8,128,512]{3,2,0,1:T(8,128)(2,1)}, u32[]{:S(2)}, u32[]{:S(2)}) %all-to-all-start.2) | async-done | bytes 1048608 | tf_op jit(solution)/shard_map/all_to_all | solution.py:140
  278.0 3.3 %gather_fusion.2 = bf16[512,512]{1,0:T(8,128)(2,1)S(1)} fusion(bf16[1024,512]{1,0:T(8,128)(2,1)} %bitcast.25, s32[1024]{0:T(1024)S(1)} %pad_clamp_fusion), kind=kCustom, calls=%fused_computation.2 | custom fusion | bytes 1050624 | tf_op jit(solution)/shard_map/jit(_take)/gather | solution.py:143
  281.6 1.8 fusion.30
  283.4 3.4 %fusion.26 = bf16[256,512]{1,0:T(8,128)(2,1)} fusion(bf16[256,2048]{1,0:T(8,128)(2,1)} %all-gather.8.cloned.1.call-done, bf16[2048,512]{1,0:T(8,128)(2,1)} %param.27, f32[256,1,512]{2,1,0:T(1,128)} %fusion.30, bf16[256,512]{1,0:T(8,128)(2,1)S(1)} %copy-done.3), kind=kOutput, calls=%fused_computation.35 | convolution fusion | flops 537395200 | bytes 4194304 | tf_op jit(solution)/shard_map/dot_general | solution.py:138
  (82 shorter events, 7.2 us)
Async XLA Ops:
  6.5 234.7 %copy-start = (bf16[1,2048,512]{2,1,0:T(8,128)(2,1)S(1)}, bf16[1,2048,512]{2,1,0:T(8,128)(2,1)}, u32[]{:S(2)}) copy-start(bf16[1,2048,512]{2,1,0:T(8,128)(2,1)} %param.24) | copy-start | bytes 6291460
  7.8 5.5 %copy-start.2 = (bf16[2,256,256]{1,2,0:T(8,128)(2,1)}, bf16[2,256,256]{1,2,0:T(8,128)(2,1)S(1)}, u32[]{:S(2)}) copy-start(bf16[2,256,256]{1,2,0:T(8,128)(2,1)S(1)} %copy.63) | copy-start | bytes 786436
  7.8 10.9 %copy-start.4 = (bf16[256,256]{1,0:T(8,128)(2,1)S(1)}, bf16[256,256]{1,0:T(8,128)(2,1)}, u32[]{:S(2)}) copy-start(bf16[256,256]{1,0:T(8,128)(2,1)} %param.14) | copy-start | bytes 393220
  7.8 11.8 %collective-permute-start = (bf16[2,128,256]{1,2,0:T(8,128)(2,1)S(1)}, bf16[2,128,256]{1,2,0:T(8,128)(2,1)}, u32[]{:S(2)}, u32[]{:S(2)}) collective-permute-start(bf16[2,128,256]{1,2,0:T(8,128)(2,1)S(1)} %slice.34), channel_id=1, source_target_pairs={{0,4},{4,8},{8,12},{12,16},{16,20},{20,24},{24,28},{1,5},{5,9},{9,... | collective-permute-start | bytes 393224 | tf_op jit(solution)/shard_map/ppermute | solution.py:20
  13.3 29.4 %all-to-all-start = ((bf16[256,4,512]{0,2,1:T(8,128)(2,1)}), bf16[256,4,512]{0,2,1:T(8,128)(2,1)S(1)}, u32[]{:S(2)}, u32[]{:S(2)}) async-start(bf16[256,4,512]{0,2,1:T(8,128)(2,1)} %bitcast.91), calls=%async_computation | async-start | bytes 2097152 | tf_op jit(solution)/shard_map/all_to_all | solution.py:81
  17.8 54.0 %all-gather.6.cloned.1.call-start = ((), (), s32[]{:S(2)}) async-start(), calls=%async_computation.3 | async-start | bytes 1310720 | tf_op jit(solution)/shard_map/all_gather | solution.py:91
  22.0 5.6 %copy-start.6 = (pred[2,128,256]{1,2,0:T(8,128)(4,1)S(1)}, pred[2,128,256]{1,2,0:T(8,128)(4,1)}, u32[]{:S(2)}) copy-start(pred[2,128,256]{1,2,0:T(8,128)(4,1)} %broadcast_and_fusion) | copy-start | bytes 196612
  24.0 5.1 %copy-start.9 = (f32[4]{0:T(128)S(1)}, f32[4]{0:T(128)}, u32[]{:S(2)}) copy-start(f32[4]{0:T(128)} %param.16) | copy-start | bytes 52
  27.6 1.8 copy-start.5
  29.8 14.3 %copy-start.13 = (bf16[256,512]{1,0:T(8,128)(2,1)S(1)}, bf16[256,512]{1,0:T(8,128)(2,1)}, u32[]{:S(2)}) copy-start(bf16[256,512]{1,0:T(8,128)(2,1)} %param.18) | copy-start | bytes 786436
  42.7 4.0 %copy-start.7 = (s32[256,2]{0,1:T(2,128)S(1)}, s32[256,2]{0,1:T(2,128)}, u32[]{:S(2)}) copy-start(s32[256,2]{0,1:T(2,128)} %param.20) | copy-start | bytes 6148
  46.6 194.7 %all-gather.10.cloned.1.call-start = ((), (), s32[]{:S(2)}) async-start(), calls=%async_computation.5 | async-start | bytes 5242880 | tf_op jit(solution)/shard_map/all_gather | solution.py:133
  182.9 1.6 copy-start.10
  182.9 1.6 copy-start.14
  184.5 2.4 copy-start.11
  186.9 3.8 %copy-start.1 = (bf16[256,2048]{1,0:T(8,128)(2,1)S(1)}, bf16[256,2048]{1,0:T(8,128)(2,1)}, u32[]{:S(2)}) copy-start(bf16[256,2048]{1,0:T(8,128)(2,1)} %all-gather.6.cloned.1.call-done) | copy-start | bytes 3145732
  246.8 31.3 %all-to-all-start.2 = ((bf16[1,8,128,512]{3,2,0,1:T(8,128)(2,1)}), bf16[1,8,128,512]{3,2,0,1:T(8,128)(2,1)}, u32[]{:S(2)}, u32[]{:S(2)}) async-start(bf16[1,8,128,512]{3,2,0,1:T(8,128)(2,1)} %bitcast.93), calls=%async_computation.2 | async-start | bytes 2097152 | tf_op jit(solution)/shard_map/all_to_all | solution.py:140
  251.4 32.0 %all-gather.8.cloned.1.call-start = ((), (), s32[]{:S(2)}) async-start(), calls=%async_computation.4 | async-start | bytes 1310720 | tf_op jit(solution)/shard_map/all_gather | solution.py:134
  251.4 2.6 copy-start.12
  254.0 2.1 copy-start.8
  281.6 1.8 copy-start.3
Sparse Core Ops, SparseCore 0:
  46.7 25.0 all-gather.5
  190.8 50.3 all-gather.9
  255.8 26.7 all-gather.7
where the time goes:
time: 294 us; the launch traced here: 293 us
  blocking collectives  111 us (38%)
  waiting for transfers between devices  92.4 us (31%)
  local copies, waits for them, and re-layouts  30.1 us (10%)
  matrix products  25.3 us (9%)
  between operations  13.5 us (5%)
  starting transfers between devices  12.4 us (4%)
  other arithmetic  8.46 us (3%)
    all_to_all x1, blocking collectives, per_device(): lax.all_to_all(picked_rows.reshape(EXP_DEV, sp_count, capacity, stream_ro...  98.4 us
    all_gather x1, waiting for transfers between devices, per_device(): routed_piece = lax.all_gather(hidden, 'tp', axis=2, tiled=True)  50.3 us
    all_to_all x1, waiting for transfers between devices, per_device(): lax.all_to_all(outgoing, 'sp', split_axis=1, concat_axis=1, tiled=True)  21.8 us
    all_gather x1, waiting for transfers between devices, per_device(): stream_rows = lax.all_gather(stream_cols, 'tp', axis=1, tiled=True)  20.4 us
    all_gather x1, blocking collectives, per_device(): attended_all = lax.all_gather(attended_values, 'tp', axis=1, tiled=True)  12.7 us
    gather x1, local copies, waits for them, and re-layouts, per_device(): jnp.take(stream_rows, slot_owner, axis=0, mode='fill', fill_value=0)  10.2 us
  transfers between devices with their start and end apart: 6, of which 3 were waited for; matrix products, arithmetic and copies ran while one was open for 10% of the time, Pallas kernels for 0%

commit v1 on v0

--- a/solution.py
+++ b/solution.py
@@ -130,10 +130,34 @@
     shared_hidden = (jax.nn.silu(own_scale * shared_gate_sum) * (own_scale * shared_up_sum)).astype(
         jnp.bfloat16
     )
-    routed_piece = lax.all_gather(hidden, "tp", axis=2, tiled=True)
     own_piece = lax.all_gather(shared_hidden[None], "tp", axis=2, tiled=True)
-    expert_out = jnp.einsum(
-        "erf,efd->erd", routed_piece, down_weight, preferred_element_type=jnp.float32
+
+    def pair_the_surface(x_local, named_axis, local):
+        mid_arr = lax.axis_size(named_axis)
+        g_now, y1, wide_out = (mid_arr, lax.axis_index(named_axis), x_local.shape[2])
+        store = tuple(((idx, (idx + 1) % g_now) for idx in range(g_now)))
+        piece_out = g_now // 2
+        table = tuple(((idx, (idx - 1) % g_now) for idx in range(g_now)))
+        heard = local(x_local, y1 * wide_out)
+        part_now = vec_out = x_local
+        for k in range(1, piece_out + 1):
+            part_now = lax.ppermute(part_now, named_axis, store)
+            if k < g_now - piece_out:
+                vec_out = lax.ppermute(vec_out, named_axis, table)
+                latest = local(vec_out, (y1 + k) % g_now * wide_out)
+                heard = heard + latest
+            heard = heard + local(part_now, (y1 - k) % g_now * wide_out)
+        return heard
+
+    expert_out = pair_the_surface(
+        hidden,
+        "tp",
+        lambda own_block, at: jnp.einsum(
+            "erf,efd->erd",
+            own_block,
+            lax.dynamic_slice_in_dim(down_weight, at, own_block.shape[2], axis=1),
+            preferred_element_type=jnp.float32,
+        ),
     )
     shared_out = jnp.dot(own_piece[0], shared_down, preferred_element_type=jnp.float32)
     outgoing = expert_out.astype(jnp.bfloat16).reshape(EXP_DEV, sp_count, capacity, col_width)

time: 294 us -> 310 us (1.054)
  waiting for transfers between devices: 92.4 us -> 103 us
    ppermute x0 -> x3, waiting for transfers between devices: none -> 61 us  [the longest x2 43 us: pair_the_surface(): part_now = lax.ppermute(part_now, named_axis, store)]
    all_gather x1 -> x0, waiting for transfers between devices: 50.3 us -> none  [per_device(): routed_piece = lax.all_gather(hidden, 'tp', axis=2, tiled=True)]
    ppermute x0 -> x3, starting transfers between devices: none -> 3.49 us  [the longest x2 2.04 us: pair_the_surface(): part_now = lax.ppermute(part_now, named_axis, store)]
    dot_general x1 -> x4, matrix products: 5.49 us -> 7.49 us  [per_device(): jnp.einsum('erf,efd->erd', own_block, lax.dynamic_slice_in_dim(down_weigh...]
  transfers between devices with their start and end apart: 6 -> 8, of which waited for: 3 -> 5; matrix products, arithmetic and copies ran while one was open for 10% -> 11% of each run, Pallas kernels for 0% -> 0%
where the time goes in v1:
time: 310 us; the launch traced here: 309 us
  blocking collectives  111 us (36%)
  waiting for transfers between devices  103 us (33%)
  local copies, waits for them, and re-layouts  30.1 us (10%)
  matrix products  27.3 us (9%)
  starting transfers between devices  15.5 us (5%)
  between operations  13.8 us (4%)
  other arithmetic  8.46 us (3%)
    all_to_all x1, blocking collectives, per_device(): lax.all_to_all(picked_rows.reshape(EXP_DEV, sp_count, capacity, stream_ro...  98.4 us
    ppermute x2, waiting for transfers between devices, pair_the_surface(): part_now = lax.ppermute(part_now, named_axis, store)  43 us
    all_to_all x1, waiting for transfers between devices, per_device(): lax.all_to_all(outgoing, 'sp', split_axis=1, concat_axis=1, tiled=True)  21.7 us
    all_gather x1, waiting for transfers between devices, per_device(): stream_rows = lax.all_gather(stream_cols, 'tp', axis=1, tiled=True)  20.4 us
    ppermute x1, waiting for transfers between devices, pair_the_surface(): vec_out = lax.ppermute(vec_out, named_axis, table)  18 us
    all_gather x1, blocking collectives, per_device(): attended_all = lax.all_gather(attended_values, 'tp', axis=1, tiled=True)  12.7 us
    gather x1, local copies, waits for them, and re-layouts, per_device(): jnp.take(stream_rows, slot_owner, axis=0, mode='fill', fill_value=0)  10.2 us
    dot_general x4, matrix products, per_device(): jnp.einsum('erf,efd->erd', own_block, lax.dynamic_slice_in_dim(down_weigh...  7.49 us
  transfers between devices with their start and end apart: 8, of which 5 were waited for; matrix products, arithmetic and copies ran while one was open for 11% of the time, Pallas kernels for 0%

profile of v1, /device:TPU:0, one launch (start us, length us, event | category | flops | bytes accessed | tf_op | source)
XLA Modules:
  0.0 309.3 jit_solution(376400494426715132)
XLA Ops:
  6.5 1.2 copy.63
  7.8 3.2 %collective-permute-start = (bf16[2,128,256]{1,2,0:T(8,128)(2,1)S(1)}, bf16[2,128,256]{1,2,0:T(8,128)(2,1)}, u32[]{:S(2)}, u32[]{:S(2)}) collective-permute-start(bf16[2,128,256]{1,2,0:T(8,128)(2,1)S(1)} %slice.34), channel_id=1, source_target_pairs={{0,4},{4,8},{8,12},{12,16},{16,20},{20,24},{24,28},{1,5},{5,9},{9,... | collective-permute-start | bytes 393224 | tf_op jit(solution)/shard_map/ppermute | solution.py:20
  11.0 2.3 copy.73
  13.3 4.5 %all-to-all-start = ((bf16[256,4,512]{0,2,1:T(8,128)(2,1)}), bf16[256,4,512]{0,2,1:T(8,128)(2,1)S(1)}, u32[]{:S(2)}, u32[]{:S(2)}) async-start(bf16[256,4,512]{0,2,1:T(8,128)(2,1)} %bitcast.109), calls=%async_computation | async-start | bytes 2097152 | tf_op jit(solution)/shard_map/all_to_all | solution.py:81
  20.7 1.4 gather_fusion
  27.6 1.5 fusion.61
  30.0 12.7 %all_gather.9 = bf16[256,1024]{0,1:T(8,128)(2,1)} all-gather(bf16[256,256]{0,1:T(8,128)(2,1)S(1)} %bitcast.112), channel_id=1, replica_groups=mesh['sp'=8,'tp'=4] {'tp'}, dimensions={1}, use_global_device_ids=true | all-gather | bytes 655360 | tf_op jit(solution)/shard_map/all_gather | solution.py:79
  42.7 1.3 copy.74
  44.0 2.6 fusion.20
  48.9 2.4 scatter_custom_fusion
  51.4 20.4 %all-gather.4.cloned.1.call-done = bf16[256,2048]{1,0:T(8,128)(2,1)} async-done(((bf16[256,512]{1,0:T(8,128)(2,1)}), bf16[256,2048]{1,0:T(8,128)(2,1)}) %all-gather.4.cloned.1.call-update) | async-done | bytes 1048592 | tf_op jit(solution)/shard_map/all_gather | solution.py:91
  71.8 10.2 %gather_fusion.1 = bf16[1024,2048]{1,0:T(8,128)(2,1)} fusion(bf16[256,2048]{1,0:T(8,128)(2,1)} %all-gather.4.cloned.1.call-done, s32[1024]{0:T(1024)S(1)} %fusion.48), kind=kCustom, calls=%fused_computation.1 | custom fusion | bytes 8392704 | tf_op jit(solution)/shard_map/jit(_take)/gather | solution.py:112
  81.9 2.5 broadcast_select_fusion
  84.5 98.4 %all_to_all.25 = bf16[1,8,128,2048]{3,2,0,1:T(8,128)(2,1)S(1)} all-to-all(bf16[1,8,128,2048]{3,2,0,1:T(8,128)(2,1)S(1)} %broadcast_select_fusion), channel_id=1, replica_groups=mesh['sp'=8,'tp'=4] {'sp'}, dimensions={1} | all-to-all | bytes 8388608 | tf_op jit(solution)/shard_map/all_to_all | solution.py:113
  184.5 2.4 fusion.3
  186.9 3.8 %multiply_convert_fusion.6 = bf16[1024,512]{1,0:T(8,128)(2,1)} fusion(f32[1024,512]{1,0:T(8,128)S(1)} %fusion.3, bf16[1024,2048]{1,0:T(8,128)(2,1)S(1)} %bitcast.106, bf16[1,2048,512]{2,1,0:T(8,128)(2,1)S(1)} %copy-done.11, f32[2048]{0:T(1024)S(1)} %copy-done.14, f32[1024]{0:T(1024)S(1)} %rsqrt_bitcast_fusion), kind=kOutput, calls=%fused_computation.17 | convolution fusion | flops 2154823680 | bytes 9449472 | tf_op jit(solution)/shard_map/erd,edf->erf/dot_general | solution.py:123
  190.7 1.5 collective-permute-start.2
  192.1 1.5 collective-permute-start.1
  193.9 24.0 %collective-permute-done.2 = bf16[1,1024,512]{2,1,0:T(8,128)(2,1)} collective-permute-done((bf16[1,1024,512]{2,1,0:T(8,128)(2,1)}, bf16[1,1024,512]{2,1,0:T(8,128)(2,1)}, u32[]{:S(2)}, u32[]{:S(2)}) %collective-permute-start.2) | collective-permute-done | bytes 1048608 | tf_op jit(solution)/shard_map/ppermute | solution.py:144
  218.5 1.9 fusion.33
  220.4 1.9 fusion.25
  222.4 18.0 %collective-permute-done.1 = bf16[1,1024,512]{2,1,0:T(8,128)(2,1)} collective-permute-done((bf16[1,1024,512]{2,1,0:T(8,128)(2,1)}, bf16[1,1024,512]{2,1,0:T(8,128)(2,1)}, u32[]{:S(2)}, u32[]{:S(2)}) %collective-permute-start.1) | collective-permute-done | bytes 1048608 | tf_op jit(solution)/shard_map/ppermute | solution.py:146
  240.4 1.9 fusion.27
  242.3 18.9 %collective-permute-done.3 = bf16[1,1024,512]{2,1,0:T(8,128)(2,1)S(1)} collective-permute-done((bf16[1,1024,512]{2,1,0:T(8,128)(2,1)}, bf16[1,1024,512]{2,1,0:T(8,128)(2,1)S(1)}, u32[]{:S(2)}, u32[]{:S(2)}) %collective-permute-start.3) | collective-permute-done | bytes 1048608 | tf_op jit(solution)/shard_map/ppermute | solution.py:144
  261.3 1.7 add_convert_fusion
  263.0 4.2 %all-to-all-start.2 = ((bf16[1,8,128,512]{3,2,0,1:T(8,128)(2,1)}), bf16[1,8,128,512]{3,2,0,1:T(8,128)(2,1)}, u32[]{:S(2)}, u32[]{:S(2)}) async-start(bf16[1,8,128,512]{3,2,0,1:T(8,128)(2,1)} %bitcast.107), calls=%async_computation.2 | async-start | bytes 2097152 | tf_op jit(solution)/shard_map/all_to_all | solution.py:164
  267.3 2.6 fusion.18
  269.9 1.6 fusion.22
  272.1 21.7 %all-to-all-done.2 = bf16[1,8,128,512]{3,2,0,1:T(8,128)(2,1)} async-done(((bf16[1,8,128,512]{3,2,0,1:T(8,128)(2,1)}), bf16[1,8,128,512]{3,2,0,1:T(8,128)(2,1)}, u32[]{:S(2)}, u32[]{:S(2)}) %all-to-all-start.2) | async-done | bytes 1048608 | tf_op jit(solution)/shard_map/all_to_all | solution.py:164
  293.8 3.3 %gather_fusion.2 = bf16[512,512]{1,0:T(8,128)(2,1)S(1)} fusion(bf16[1024,512]{1,0:T(8,128)(2,1)} %bitcast.32, s32[1024]{0:T(1024)S(1)} %pad_clamp_fusion), kind=kCustom, calls=%fused_computation.2 | custom fusion | bytes 1050624 | tf_op jit(solution)/shard_map/jit(_take)/gather | solution.py:167
  297.3 1.8 fusion.39
  299.1 3.4 %fusion.21 = bf16[256,512]{1,0:T(8,128)(2,1)} fusion(bf16[256,2048]{1,0:T(8,128)(2,1)} %all-gather.6.cloned.1.call-done, bf16[2048,512]{1,0:T(8,128)(2,1)} %param.27, f32[256,1,512]{2,1,0:T(1,128)} %fusion.39, bf16[256,512]{1,0:T(8,128)(2,1)S(1)} %copy-done.3), kind=kOutput, calls=%fused_computation.33 | convolution fusion | flops 537395200 | bytes 4194304 | tf_op jit(solution)/shard_map/dot_general | solution.py:162
  (88 shorter events, 14.9 us)
Async XLA Ops:
  6.5 212.0 %copy-start = (bf16[1,2048,512]{2,1,0:T(8,128)(2,1)S(1)}, bf16[1,2048,512]{2,1,0:T(8,128)(2,1)}, u32[]{:S(2)}) copy-start(bf16[1,2048,512]{2,1,0:T(8,128)(2,1)} %param.24) | copy-start | bytes 6291460
  7.8 5.5 %copy-start.2 = (bf16[2,256,256]{1,2,0:T(8,128)(2,1)}, bf16[2,256,256]{1,2,0:T(8,128)(2,1)S(1)}, u32[]{:S(2)}) copy-start(bf16[2,256,256]{1,2,0:T(8,128)(2,1)S(1)} %copy.63) | copy-start | bytes 786436
  7.8 10.9 %copy-start.4 = (bf16[256,256]{1,0:T(8,128)(2,1)S(1)}, bf16[256,256]{1,0:T(8,128)(2,1)}, u32[]{:S(2)}) copy-start(bf16[256,256]{1,0:T(8,128)(2,1)} %param.14) | copy-start | bytes 393220
  7.8 11.8 %collective-permute-start = (bf16[2,128,256]{1,2,0:T(8,128)(2,1)S(1)}, bf16[2,128,256]{1,2,0:T(8,128)(2,1)}, u32[]{:S(2)}, u32[]{:S(2)}) collective-permute-start(bf16[2,128,256]{1,2,0:T(8,128)(2,1)S(1)} %slice.34), channel_id=1, source_target_pairs={{0,4},{4,8},{8,12},{12,16},{16,20},{20,24},{24,28},{1,5},{5,9},{9,... | collective-permute-start | bytes 393224 | tf_op jit(solution)/shard_map/ppermute | solution.py:20
  13.3 29.4 %all-to-all-start = ((bf16[256,4,512]{0,2,1:T(8,128)(2,1)}), bf16[256,4,512]{0,2,1:T(8,128)(2,1)S(1)}, u32[]{:S(2)}, u32[]{:S(2)}) async-start(bf16[256,4,512]{0,2,1:T(8,128)(2,1)} %bitcast.109), calls=%async_computation | async-start | bytes 2097152 | tf_op jit(solution)/shard_map/all_to_all | solution.py:81
  17.8 54.0 %all-gather.4.cloned.1.call-start = ((), (), s32[]{:S(2)}) async-start(), calls=%async_computation.3 | async-start | bytes 1310720 | tf_op jit(solution)/shard_map/all_gather | solution.py:91
  22.0 5.6 %copy-start.6 = (pred[2,128,256]{1,2,0:T(8,128)(4,1)S(1)}, pred[2,128,256]{1,2,0:T(8,128)(4,1)}, u32[]{:S(2)}) copy-start(pred[2,128,256]{1,2,0:T(8,128)(4,1)} %broadcast_and_fusion) | copy-start | bytes 196612
  24.0 5.1 %copy-start.9 = (f32[4]{0:T(128)S(1)}, f32[4]{0:T(128)}, u32[]{:S(2)}) copy-start(f32[4]{0:T(128)} %param.16) | copy-start | bytes 52
  27.6 1.8 copy-start.5
  29.8 14.3 %copy-start.13 = (bf16[256,512]{1,0:T(8,128)(2,1)S(1)}, bf16[256,512]{1,0:T(8,128)(2,1)}, u32[]{:S(2)}) copy-start(bf16[256,512]{1,0:T(8,128)(2,1)} %param.18) | copy-start | bytes 786436
  42.7 3.9 %copy-start.7 = (s32[256,2]{0,1:T(2,128)S(1)}, s32[256,2]{0,1:T(2,128)}, u32[]{:S(2)}) copy-start(s32[256,2]{0,1:T(2,128)} %param.20) | copy-start | bytes 6148
  182.9 1.6 copy-start.10
  182.9 1.6 copy-start.14
  184.5 2.4 copy-start.11
  186.9 6.7 %copy-start.1 = (bf16[256,2048]{1,0:T(8,128)(2,1)S(1)}, bf16[256,2048]{1,0:T(8,128)(2,1)}, u32[]{:S(2)}) copy-start(bf16[256,2048]{1,0:T(8,128)(2,1)} %all-gather.4.cloned.1.call-done) | copy-start | bytes 3145732
  190.7 27.2 %collective-permute-start.2 = (bf16[1,1024,512]{2,1,0:T(8,128)(2,1)}, bf16[1,1024,512]{2,1,0:T(8,128)(2,1)}, u32[]{:S(2)}, u32[]{:S(2)}) collective-permute-start(bf16[1,1024,512]{2,1,0:T(8,128)(2,1)} %bitcast.23), channel_id=1, source_target_pairs={{0,1},{1,2},{2,3},{3,0},{4,5},{5,6},{6,7},{7,4},{8,9},{9,10},{10,1... | collective-permute-start | bytes 3145736 | tf_op jit(solution)/shard_map/ppermute | solution.py:144
  192.1 48.3 %collective-permute-start.1 = (bf16[1,1024,512]{2,1,0:T(8,128)(2,1)}, bf16[1,1024,512]{2,1,0:T(8,128)(2,1)}, u32[]{:S(2)}, u32[]{:S(2)}) collective-permute-start(bf16[1,1024,512]{2,1,0:T(8,128)(2,1)} %bitcast.23), channel_id=1, source_target_pairs={{0,3},{1,0},{2,1},{3,2},{4,7},{5,4},{6,5},{7,6},{8,11},{9,8},{10,9... | collective-permute-start | bytes 3145736 | tf_op jit(solution)/shard_map/ppermute | solution.py:146
  217.9 43.3 %collective-permute-start.3 = (bf16[1,1024,512]{2,1,0:T(8,128)(2,1)}, bf16[1,1024,512]{2,1,0:T(8,128)(2,1)S(1)}, u32[]{:S(2)}, u32[]{:S(2)}) collective-permute-start(bf16[1,1024,512]{2,1,0:T(8,128)(2,1)} %collective-permute-done.2), channel_id=1, source_target_pairs={{0,1},{1,2},{2,3},{3,0},{4,5},{5,6},{6,7},{7,4},{8,9},{9,10},{10,1... | collective-permute-start | bytes 3145736 | tf_op jit(solution)/shard_map/ppermute | solution.py:144
  263.0 30.8 %all-to-all-start.2 = ((bf16[1,8,128,512]{3,2,0,1:T(8,128)(2,1)}), bf16[1,8,128,512]{3,2,0,1:T(8,128)(2,1)}, u32[]{:S(2)}, u32[]{:S(2)}) async-start(bf16[1,8,128,512]{3,2,0,1:T(8,128)(2,1)} %bitcast.107), calls=%async_computation.2 | async-start | bytes 2097152 | tf_op jit(solution)/shard_map/all_to_all | solution.py:164
  267.2 31.9 %all-gather.6.cloned.1.call-start = ((), (), s32[]{:S(2)}) async-start(), calls=%async_computation.4 | async-start | bytes 1310720 | tf_op jit(solution)/shard_map/all_gather | solution.py:133
  267.3 2.6 copy-start.12
  269.8 2.1 copy-start.8
  297.3 1.8 copy-start.3
Sparse Core Ops, SparseCore 0:
  46.7 24.9 all-gather.3
  271.6 26.6 all-gather.5
